TPU v7x, 32 devices: a whole 2x2x4 slice. The times are simulated.
32 devices in a mesh: grp: 2 (over y), fs: 8 (over z, core), tp: 2 (over x).
Axes of the slice: x: 2, y: 2, z: 4, core: 2. Of those that a mesh axis runs over, the one named last changes fastest.
Arguments:
- prompt: bfloat16 [6144, 2048], P(('grp', 'fs')), parts along dimension 0, may hold values from -6 to 6
- routes: int32 [6144, 4], P(('grp', 'fs')), parts along dimension 0, may hold values from 0 to 7, all different within a row; in each aligned block of 384 rows (0 to 383, 384 to 767, ...) at most 240 rows name the same one
- route_weight: float32 [6144, 4], P(('grp', 'fs')), parts along dimension 0, may hold values from 0.2 to 1
- norm_gain: float32 [2048], P('fs'), may hold values from 0.1 to 1.9
- gate_train: float32 [8, 2048, 1024], P(None, 'fs', 'tp'), may hold values from -0.4 to 0.4
- up_train: float32 [8, 2048, 1024], P(None, 'fs', 'tp'), may hold values from -0.4 to 0.4
- down_train: float32 [8, 1024, 2048], P(None, 'fs', 'tp'), may hold values from -0.07 to 0.07
Outputs:
- gate_serve: bfloat16 [16, 2048, 1024], P(('grp', 'fs'), None, 'tp'), parts along dimension 0
- up_serve: bfloat16 [16, 2048, 1024], P(('grp', 'fs'), None, 'tp'), parts along dimension 0
- down_serve: bfloat16 [16, 1024, 2048], P(('grp', 'fs'), 'tp'), parts along dimension 0
- mixed: bfloat16 [6144, 2048], P(('grp', 'fs'), 'tp'), parts along dimension 0
There are 2 independent parts, one for each index of `grp`. A program takes and returns all parts, laid end to end along the dimension named above; an argument that names none is the same for every part. Nothing has to cross between parts.
Inputs may be any that keep to these rules, and one draw needn't show every extreme that they name: `routes`: each row names 4 different experts. Among the rows of one index of fs no expert is named more than 240 times, a bound that some block reaches on some index.
All inputs are finite; a program needn't handle non-finite values.
Results may differ from a plain program's by a relative error of at most 0.012.
Values may be sent and summed in bfloat16 or wider, within the bound.
A program may use at most 128 MiB of HBM per device.

v0:
```python
import jax
import jax.numpy as jnp
from jax import lax
from jax.sharding import PartitionSpec as P

LIMIT = 7.0
ALPHA = 1.702
EPS = 1e-06


def shards(prompt, routes, route_weight, norm_gain, gate_train, up_train, down_train):
    tp = lax.axis_size("tp")
    experts = gate_train.shape[0]
    tok_rows, width = prompt.shape
    values = prompt.astype(jnp.float32)
    normed = (values * lax.rsqrt(jnp.mean(values * values, axis=-1, keepdims=True) + EPS)).astype(
        jnp.bfloat16
    )
    lanes = jnp.arange(experts, dtype=jnp.int32)
    scale = jnp.sum(
        jnp.where(routes[:, :, None] == lanes[None, None, :], route_weight[:, :, None], 0.0), axis=1
    )
    scale = lax.all_to_all(scale.T, "fs", split_axis=0, concat_axis=0, tiled=True)
    scale = scale.reshape(-1, 1)
    tokens = lax.all_gather(normed, "fs", axis=0, tiled=True)
    gain = norm_gain[None, :, None]
    gate_mine = lax.all_to_all(
        (gain * gate_train).astype(jnp.bfloat16), "fs", split_axis=0, concat_axis=0, tiled=True
    ).reshape(width, -1)
    up_mine = lax.all_to_all(
        (gain * up_train).astype(jnp.bfloat16), "fs", split_axis=0, concat_axis=0, tiled=True
    ).reshape(width, -1)
    down_rows = lax.all_to_all(
        down_train.astype(jnp.bfloat16), "fs", split_axis=0, concat_axis=0, tiled=True
    )
    down_rows = down_rows.reshape(-1, down_rows.shape[2])
    cols = down_rows.shape[1]
    own = gate_mine.shape[1]
    down_mine = lax.all_to_all(down_rows, "tp", split_axis=0, concat_axis=0, tiled=True)
    down_mine = down_mine.reshape(tp, own, cols).transpose(1, 0, 2).reshape(own, tp * cols)
    gate_pre = jnp.minimum(jnp.dot(tokens, gate_mine, preferred_element_type=jnp.float32), LIMIT)
    up_pre = jnp.clip(jnp.dot(tokens, up_mine, preferred_element_type=jnp.float32), -LIMIT, LIMIT)
    hidden = ((up_pre + 1.0) * gate_pre * jax.nn.sigmoid(ALPHA * gate_pre)).astype(jnp.bfloat16)
    pieces = lax.all_gather(hidden, "tp", axis=0, tiled=True)
    total = jnp.zeros((hidden.shape[0], cols), jnp.float32)
    for index in range(tp):
        total = total + jnp.dot(
            pieces[index * hidden.shape[0] : (index + 1) * hidden.shape[0]],
            down_rows[index * own : (index + 1) * own],
            preferred_element_type=jnp.float32,
        )
    weighted = (total * scale).astype(jnp.bfloat16)
    mixed = lax.psum_scatter(weighted, "fs", scatter_dimension=0, tiled=True)
    return (gate_mine[None], up_mine[None], down_mine[None], mixed)


def solution(mesh):
    return jax.shard_map(
        shards,
        mesh=mesh,
        in_specs=(
            P(("grp", "fs"), None),
            P(("grp", "fs"), None),
            P(("grp", "fs"), None),
            P("fs"),
            P(None, "fs", "tp"),
            P(None, "fs", "tp"),
            P(None, "fs", "tp"),
        ),
        out_specs=(
            P(("grp", "fs"), None, "tp"),
            P(("grp", "fs"), None, "tp"),
            P(("grp", "fs"), "tp", None),
            P(("grp", "fs"), "tp"),
        ),
        check_vma=False,
    )
```

profile of v0, /device:TPU:0, one launch (start us, length us, event | category | flops | bytes accessed | tf_op | source)
XLA Modules:
  0.0 429.3 jit_solution(14613814790445612276)
XLA Ops:
  7.2 1.8 fusion
  9.0 2.9 fusion.1
  11.9 6.1 %multiply_convert_fusion.2 = (bf16[8,256,512]{2,1,0:T(8,128)(2,1)}, bf16[8,256,512]{2,1,0:T(8,128)(2,1)S(1)}) fusion(f32[8,256,512]{2,1,0:T(8,128)} %param.12, f32[256]{0:T(256)S(1)} %copy-done.2, f32[8,256,512]{2,1,0:T(8,128)} %param.11), kind=kLoop, calls=%fused_computation.2 | loop fusion | flops 4194304 | bytes 12583936 | tf_op jit(solution)/shard_map/convert_element_type | solution.py:31
  18.1 111.5 %all_to_all.33 = bf16[8,256,512]{2,1,0:T(8,128)(2,1)S(1)} all-to-all(bf16[8,256,512]{2,1,0:T(8,128)(2,1)S(1)} %get-tuple-element.15), channel_id=1, replica_groups=mesh['grp'=2,'fs'=8,'tp'=2] {'fs'}, dimensions={0} | all-to-all | bytes 4194304 | tf_op jit(solution)/shard_map/all_to_all | solution.py:27
  129.6 4.3 %all-to-all-start.1 = ((bf16[8,256,512]{2,1,0:T(8,128)(2,1)}), bf16[8,256,512]{2,1,0:T(8,128)(2,1)}, u32[]{:S(2)}, u32[]{:S(2)}) async-start(bf16[8,256,512]{2,1,0:T(8,128)(2,1)} %get-tuple-element.14), calls=%async_computation.1 | async-start | bytes 4194304 | tf_op jit(solution)/shard_map/all_to_all | solution.py:30
  134.0 87.0 %all-gather.3.cloned.1.call-done = bf16[3072,2048]{1,0:T(8,128)(2,1)} async-done(((bf16[384,2048]{1,0:T(8,128)(2,1)}), bf16[3072,2048]{1,0:T(8,128)(2,1)}) %all-gather.3.cloned.1.call-update) | async-done | bytes 12582928 | tf_op jit(solution)/shard_map/all_gather | solution.py:25
  221.0 11.4 %fusion.6 = f32[3072,512]{1,0:T(8,128)} fusion(bf16[3072,2048]{1,0:T(8,128)(2,1)} %all-gather.3.cloned.1.call-done, bf16[2048,512]{1,0:T(8,128)(2,1)S(1)} %bitcast.20), kind=kOutput, calls=%fused_computation.15 | convolution fusion | flops 6442450944 | bytes 20971520 | tf_op jit(solution)/shard_map/dot_general | solution.py:41
  232.4 15.8 %multiply_convert_fusion.1 = bf16[3072,512]{1,0:T(8,128)(2,1)} fusion(f32[3072,512]{1,0:T(8,128)} %fusion.6, bf16[3072,2048]{1,0:T(8,128)(2,1)} %all-gather.3.cloned.1.call-done, bf16[2048,512]{1,0:T(8,128)(2,1)} %bitcast.5), kind=kOutput, calls=%fused_computation.1 | convolution fusion | flops 6458179584 | bytes 24117248 | tf_op jit(solution)/shard_map/dot_general | solution.py:42
  248.2 3.8 convert_element_type.23
  252.0 4.4 %all-to-all-start.2 = ((bf16[8,128,1024]{2,1,0:T(8,128)(2,1)}), bf16[8,128,1024]{2,1,0:T(8,128)(2,1)}, u32[]{:S(2)}, u32[]{:S(2)}) async-start(bf16[8,128,1024]{2,1,0:T(8,128)(2,1)} %convert_element_type.23), calls=%async_computation.2 | async-start | bytes 4194304 | tf_op jit(solution)/shard_map/all_to_all | solution.py:33
  256.4 0.6 copy.24
  257.1 48.4 %all-to-all-done.2 = bf16[8,128,1024]{2,1,0:T(8,128)(2,1)} async-done(((bf16[8,128,1024]{2,1,0:T(8,128)(2,1)}), bf16[8,128,1024]{2,1,0:T(8,128)(2,1)}, u32[]{:S(2)}, u32[]{:S(2)}) %all-to-all-start.2) | async-done | bytes 2097184 | tf_op jit(solution)/shard_map/all_to_all | solution.py:33
  305.4 3.3 all-to-all-start.4
  309.0 2.8 fusion.5
  311.8 15.0 %all-gather.5.cloned.1.call-done = bf16[6144,512]{1,0:T(8,128)(2,1)} async-done(((bf16[3072,512]{1,0:T(8,128)(2,1)}), bf16[6144,512]{1,0:T(8,128)(2,1)}) %all-gather.5.cloned.1.call-update) | async-done | bytes 6291472 | tf_op jit(solution)/shard_map/all_gather | solution.py:44
  326.8 10.1 %fusion.3 = f32[3072,1024]{1,0:T(8,128)} fusion(bf16[512,1024]{1,0:T(8,128)(2,1)} %bitcast.24, bf16[6144,512]{1,0:T(8,128)(2,1)} %all-gather.5.cloned.1.call-done), kind=kOutput, calls=%fused_computation.9 | convolution fusion | flops 3221225472 | bytes 16777216 | tf_op jit(solution)/shard_map/dot_general | solution.py:47
  336.9 11.6 %multiply_convert_fusion = bf16[3072,1024]{1,0:T(8,128)(2,1)} fusion(f32[3072,1024]{1,0:T(8,128)} %fusion.3, f32[3072]{0:T(1024)S(1)} %bitcast.26, bf16[512,1024]{1,0:T(8,128)(2,1)S(1)} %bitcast.23, bf16[6144,512]{1,0:T(8,128)(2,1)} %all-gather.5.cloned.1.call-done), kind=kOutput, calls=%fused_computation | convolution fusion | flops 3230662656 | bytes 23080960 | tf_op jit(solution)/shard_map/dot_general | solution.py:47
  348.6 4.8 %all-to-all-start.3 = ((bf16[2,512,1024]{2,1,0:T(8,128)(2,1)}), bf16[2,512,1024]{2,1,0:T(8,128)(2,1)}, u32[]{:S(2)}, u32[]{:S(2)}) async-start(bf16[2,512,1024]{2,1,0:T(8,128)(2,1)} %bitcast.2), calls=%async_computation.3 | async-start | bytes 4194304 | tf_op jit(solution)/shard_map/all_to_all | solution.py:39
  353.4 25.0 %all-to-all-done.3 = bf16[2,512,1024]{2,1,0:T(8,128)(2,1)} async-done(((bf16[2,512,1024]{2,1,0:T(8,128)(2,1)}), bf16[2,512,1024]{2,1,0:T(8,128)(2,1)}, u32[]{:S(2)}, u32[]{:S(2)}) %all-to-all-start.3) | async-done | bytes 2097184 | tf_op jit(solution)/shard_map/all_to_all | solution.py:39
  378.4 4.0 copy.23
  382.4 3.9 copy.25
  386.3 32.1 %reduce-scatter.2.cloned.1.call-done = bf16[384,1024]{1,0:T(8,128)(2,1)} async-done(((bf16[3072,1024]{1,0:T(8,128)(2,1)}), bf16[384,1024]{1,0:T(8,128)(2,1)}) %reduce-scatter.2.cloned.1.call-update) | async-done | bytes 786448 | tf_op jit(solution)/shard_map/reduce_scatter | solution.py:53
  418.4 1.3 copy.28
  419.8 3.0 copy.29
  (16 shorter events, 0.4 us)
Async XLA Ops:
  7.2 4.8 %copy-start.2 = (f32[256]{0:T(256)S(1)}, f32[256]{0:T(256)}, u32[]{:S(2)}) copy-start(f32[256]{0:T(256)} %param.10) | copy-start | bytes 3076
  7.2 213.8 %all-gather.3.cloned.1.call-start = ((), (), s32[]{:S(2)}) async-start(), calls=%async_computation.6 | async-start | bytes 14155776 | tf_op jit(solution)/shard_map/all_gather | solution.py:25
  129.6 102.8 %all-to-all-start.1 = ((bf16[8,256,512]{2,1,0:T(8,128)(2,1)}), bf16[8,256,512]{2,1,0:T(8,128)(2,1)}, u32[]{:S(2)}, u32[]{:S(2)}) async-start(bf16[8,256,512]{2,1,0:T(8,128)(2,1)} %get-tuple-element.14), calls=%async_computation.1 | async-start | bytes 4194304 | tf_op jit(solution)/shard_map/all_to_all | solution.py:30
  133.9 192.8 %all-gather.5.cloned.1.call-start = ((), (), s32[]{:S(2)}) async-start(), calls=%async_computation.7 | async-start | bytes 9437184 | tf_op jit(solution)/shard_map/all_gather | solution.py:44
  248.1 8.3 %copy-start = (f32[384,4]{0,1:T(4,128)S(1)}, f32[384,4]{0,1:T(4,128)}, u32[]{:S(2)}) copy-start(f32[384,4]{0,1:T(4,128)} %param.9) | copy-start | bytes 18436
  248.1 8.3 %copy-start.1 = (s32[384,4]{0,1:T(4,128)S(1)}, s32[384,4]{0,1:T(4,128)}, u32[]{:S(2)}) copy-start(s32[384,4]{0,1:T(4,128)} %param.8) | copy-start | bytes 18436
  252.0 53.4 %all-to-all-start.2 = ((bf16[8,128,1024]{2,1,0:T(8,128)(2,1)}), bf16[8,128,1024]{2,1,0:T(8,128)(2,1)}, u32[]{:S(2)}, u32[]{:S(2)}) async-start(bf16[8,128,1024]{2,1,0:T(8,128)(2,1)} %convert_element_type.23), calls=%async_computation.2 | async-start | bytes 4194304 | tf_op jit(solution)/shard_map/all_to_all | solution.py:33
  305.4 31.5 %all-to-all-start.4 = ((f32[8,1,384]{2,1,0:T(1,128)}), f32[8,1,384]{2,1,0:T(1,128)S(1)}, u32[]{:S(2)}, u32[]{:S(2)}) async-start(f32[8,1,384]{2,1,0:T(1,128)} %copy.24), calls=%async_computation.4 | async-start | bytes 24576 | tf_op jit(solution)/shard_map/all_to_all | solution.py:23
  308.8 109.7 %reduce-scatter.2.cloned.1.call-start = ((), (), s32[]{:S(2)}) async-start(), calls=%async_computation.8 | async-start | bytes 7077888 | tf_op jit(solution)/shard_map/reduce_scatter | solution.py:53
  348.6 29.9 %all-to-all-start.3 = ((bf16[2,512,1024]{2,1,0:T(8,128)(2,1)}), bf16[2,512,1024]{2,1,0:T(8,128)(2,1)}, u32[]{:S(2)}, u32[]{:S(2)}) async-start(bf16[2,512,1024]{2,1,0:T(8,128)(2,1)} %bitcast.2), calls=%async_computation.3 | async-start | bytes 4194304 | tf_op jit(solution)/shard_map/all_to_all | solution.py:39
Sparse Core Ops, SparseCore 0:
  12.0 208.8 all-gather.2
  248.3 78.4 all-gather.4
  348.7 69.7 reduce-scatter.1
where the time goes:
time: 430 us; the launch traced here: 429 us
  waiting for transfers between devices  208 us (48%)
  blocking collectives  112 us (26%)
  matrix products  48.9 us (11%)
  starting transfers between devices  17.2 us (4%)
  local copies, waits for them, and re-layouts  15.6 us (4%)
  other arithmetic  14.7 us (3%)
  between operations  13.8 us (3%)
    all_to_all x1, blocking collectives, shards(): lax.all_to_all((gain * gate_train).astype(jnp.bfloat16), 'fs', split_axis...  112 us
    all_gather x1, waiting for transfers between devices, shards(): tokens = lax.all_gather(normed, 'fs', axis=0, tiled=True)  87 us
    all_to_all x1, waiting for transfers between devices, shards(): lax.all_to_all(down_train.astype(jnp.bfloat16), 'fs', split_axis=0, conca...  48.4 us
    reduce_scatter x1, waiting for transfers between devices, shards(): mixed = lax.psum_scatter(weighted, 'fs', scatter_dimension=0, tiled=True)  32.1 us
    all_to_all x1, waiting for transfers between devices, shards(): lax.all_to_all(down_rows, 'tp', split_axis=0, concat_axis=0, tiled=True)  25 us
    dot_general x2, matrix products, shards(): jnp.dot(pieces[index * hidden.shape[0]:(index + 1) * hidden.shape[0]], do...  21.8 us
    dot_general x1, matrix products, shards(): jnp.dot(tokens, up_mine, preferred_element_type=jnp.float32)  15.8 us
    all_gather x1, waiting for transfers between devices, shards(): pieces = lax.all_gather(hidden, 'tp', axis=0, tiled=True)  15 us
  transfers between devices with their start and end apart: 7, of which 5 were waited for; matrix products, arithmetic and copies ran while one was open for 10% of the time, Pallas kernels for 0%

commit v1 on v0

--- a/solution.py
+++ b/solution.py
@@ -22,7 +22,10 @@
     )
     scale = lax.all_to_all(scale.T, "fs", split_axis=0, concat_axis=0, tiled=True)
     scale = scale.reshape(-1, 1)
-    tokens = lax.all_gather(normed, "fs", axis=0, tiled=True)
+    peers = lax.axis_size("fs")
+    tiles = jnp.stack([normed for _ in range(peers)])
+    tiles = lax.all_to_all(tiles, "fs", split_axis=0, concat_axis=0)
+    tokens = jnp.concatenate(tiles, axis=0)
     gain = norm_gain[None, :, None]
     gate_mine = lax.all_to_all(
         (gain * gate_train).astype(jnp.bfloat16), "fs", split_axis=0, concat_axis=0, tiled=True

time: 430 us -> 610 us (1.42)
  blocking collectives: 112 us -> 280 us
  local copies, waits for them, and re-layouts: 15.6 us -> 23.3 us
  starting transfers between devices: 17.2 us -> 23.5 us
    all_to_all x1, blocking collectives: 112 us -> 280 us  [shards(): tiles = lax.all_to_all(tiles, 'fs', split_axis=0, concat_axis=0)]
    all_gather x1 -> x0, waiting for transfers between devices: 87 us -> none  [shards(): tokens = lax.all_gather(normed, 'fs', axis=0, tiled=True)]
    all_to_all x0 -> x1, waiting for transfers between devices: none -> 44.4 us  [shards(): lax.all_to_all((gain * gate_train).astype(jnp.bfloat16), 'fs', split_axis...]
    all_to_all x1, waiting for transfers between devices: 0.01 us -> 37.6 us  [shards(): lax.all_to_all((gain * up_train).astype(jnp.bfloat16), 'fs', split_axis=0...]
    another operation x0 -> x1, local copies, waits for them, and re-layouts: none -> 7.64 us  [shards(): tiles = jnp.stack([normed for _ in range(peers)])]
    all_to_all x0 -> x1, starting transfers between devices: none -> 6.35 us  [shards(): lax.all_to_all((gain * gate_train).astype(jnp.bfloat16), 'fs', split_axis...]
  transfers between devices with their start and end apart: 7 -> 7, of which waited for: 5 -> 6; matrix products, arithmetic and copies ran while one was open for 10% -> 7% of each run, Pallas kernels for 0% -> 0%
where the time goes in v1:
time: 610 us; the launch traced here: 609 us
  blocking collectives  280 us (46%)
  waiting for transfers between devices  203 us (33%)
  matrix products  48.9 us (8%)
  starting transfers between devices  23.5 us (4%)
  local copies, waits for them, and re-layouts  23.3 us (4%)
  other arithmetic  15.4 us (3%)
  between operations  14.1 us (2%)
    all_to_all x1, blocking collectives, shards(): tiles = lax.all_to_all(tiles, 'fs', split_axis=0, concat_axis=0)  280 us
    all_to_all x1, waiting for transfers between devices, shards(): lax.all_to_all(down_train.astype(jnp.bfloat16), 'fs', split_axis=0, conca...  48.4 us
    all_to_all x1, waiting for transfers between devices, shards(): lax.all_to_all((gain * gate_train).astype(jnp.bfloat16), 'fs', split_axis...  44.4 us
    all_to_all x1, waiting for transfers between devices, shards(): lax.all_to_all((gain * up_train).astype(jnp.bfloat16), 'fs', split_axis=0...  37.6 us
    reduce_scatter x1, waiting for transfers between devices, shards(): mixed = lax.psum_scatter(weighted, 'fs', scatter_dimension=0, tiled=True)  32.1 us
    all_to_all x1, waiting for transfers between devices, shards(): lax.all_to_all(down_rows, 'tp', split_axis=0, concat_axis=0, tiled=True)  25 us
    dot_general x2, matrix products, shards(): jnp.dot(pieces[index * hidden.shape[0]:(index + 1) * hidden.shape[0]], do...  21.8 us
    all_gather x1, waiting for transfers between devices, shards(): pieces = lax.all_gather(hidden, 'tp', axis=0, tiled=True)  15.8 us
  transfers between devices with their start and end apart: 7, of which 6 were waited for; matrix products, arithmetic and copies ran while one was open for 7% of the time, Pallas kernels for 0%

profile of v1, /device:TPU:0, one launch (start us, length us, event | category | flops | bytes accessed | tf_op | source)
XLA Modules:
  0.0 608.9 jit_solution(6116758632087873872)
XLA Ops:
  7.2 6.8 %multiply_convert_fusion.2 = (bf16[8,256,512]{2,1,0:T(8,128)(2,1)}, bf16[8,256,512]{2,1,0:T(8,128)(2,1)}) fusion(f32[8,256,512]{2,1,0:T(8,128)} %param.12, f32[256]{0:T(256)} %param.10, f32[8,256,512]{2,1,0:T(8,128)} %param.11), kind=kLoop, calls=%fused_computation.2 | loop fusion | flops 4194304 | bytes 12583936 | tf_op jit(solution)/shard_map/convert_element_type | solution.py:34
  14.0 6.4 %all-to-all-start = ((bf16[8,256,512]{2,1,0:T(8,128)(2,1)}), bf16[8,256,512]{2,1,0:T(8,128)(2,1)S(1)}, u32[]{:S(2)}, u32[]{:S(2)}) async-start(bf16[8,256,512]{2,1,0:T(8,128)(2,1)} %get-tuple-element.15), calls=%async_computation | async-start | bytes 4194304 | tf_op jit(solution)/shard_map/all_to_all | solution.py:30
  22.1 2.9 fusion.1
  25.0 44.4 %all-to-all-done = bf16[8,256,512]{2,1,0:T(8,128)(2,1)S(1)} async-done(((bf16[8,256,512]{2,1,0:T(8,128)(2,1)}), bf16[8,256,512]{2,1,0:T(8,128)(2,1)S(1)}, u32[]{:S(2)}, u32[]{:S(2)}) %all-to-all-start) | async-done | bytes 2097184 | tf_op jit(solution)/shard_map/all_to_all | solution.py:30
  69.4 7.6 %stack.2 = bf16[8,384,2048]{2,1,0:T(8,128)(2,1)} broadcast(bf16[384,2048]{1,0:T(8,128)(2,1)} %fusion.1), dimensions={1,2} | broadcast | bytes 14155776 | tf_op jit(solution)/shard_map/stack | solution.py:26
  77.0 280.5 %all_to_all.38 = bf16[8,384,2048]{2,1,0:T(8,128)(2,1)} all-to-all(bf16[8,384,2048]{2,1,0:T(8,128)(2,1)} %stack.2), channel_id=1, replica_groups=mesh['grp'=2,'fs'=8,'tp'=2] {'fs'}, dimensions={0} | all-to-all | bytes 25165824 | tf_op jit(solution)/shard_map/all_to_all | solution.py:27
  357.5 4.4 all-to-all-start.1
  361.9 11.4 %fusion.6 = f32[3072,512]{1,0:T(8,128)} fusion(bf16[3072,2048]{1,0:T(8,128)(2,1)} %bitcast.21, bf16[2048,512]{1,0:T(8,128)(2,1)S(1)} %bitcast.23), kind=kOutput, calls=%fused_computation.15 | convolution fusion | flops 6442450944 | bytes 20971520 | tf_op jit(solution)/shard_map/dot_general | solution.py:44
  373.3 37.6 %all-to-all-done.1 = bf16[8,256,512]{2,1,0:T(8,128)(2,1)} async-done(((bf16[8,256,512]{2,1,0:T(8,128)(2,1)}), bf16[8,256,512]{2,1,0:T(8,128)(2,1)}, u32[]{:S(2)}, u32[]{:S(2)}) %all-to-all-start.1) | async-done | bytes 2097184 | tf_op jit(solution)/shard_map/all_to_all | solution.py:33
  410.9 15.7 %multiply_convert_fusion.1 = bf16[3072,512]{1,0:T(8,128)(2,1)} fusion(f32[3072,512]{1,0:T(8,128)} %fusion.6, bf16[3072,2048]{1,0:T(8,128)(2,1)} %bitcast.22, bf16[2048,512]{1,0:T(8,128)(2,1)} %bitcast.6), kind=kOutput, calls=%fused_computation.1 | convolution fusion | flops 6458179584 | bytes 24117248 | tf_op jit(solution)/shard_map/dot_general | solution.py:45
  426.7 3.8 convert_element_type.23
  430.5 4.4 all-to-all-start.2
  435.6 48.4 %all-to-all-done.2 = bf16[8,128,1024]{2,1,0:T(8,128)(2,1)} async-done(((bf16[8,128,1024]{2,1,0:T(8,128)(2,1)}), bf16[8,128,1024]{2,1,0:T(8,128)(2,1)}, u32[]{:S(2)}, u32[]{:S(2)}) %all-to-all-start.2) | async-done | bytes 2097184 | tf_op jit(solution)/shard_map/all_to_all | solution.py:36
  483.9 3.3 all-to-all-start.5
  487.5 2.8 fusion.5
  490.3 15.8 %all-gather.2.cloned.1.call-done = bf16[6144,512]{1,0:T(8,128)(2,1)} async-done(((bf16[3072,512]{1,0:T(8,128)(2,1)}), bf16[6144,512]{1,0:T(8,128)(2,1)}) %all-gather.2.cloned.1.call-update) | async-done | bytes 6291472 | tf_op jit(solution)/shard_map/all_gather | solution.py:47
  506.1 10.1 %fusion.3 = f32[3072,1024]{1,0:T(8,128)} fusion(bf16[512,1024]{1,0:T(8,128)(2,1)} %bitcast.27, bf16[6144,512]{1,0:T(8,128)(2,1)} %all-gather.2.cloned.1.call-done), kind=kOutput, calls=%fused_computation.9 | convolution fusion | flops 3221225472 | bytes 16777216 | tf_op jit(solution)/shard_map/dot_general | solution.py:50
  516.2 11.6 %multiply_convert_fusion = bf16[3072,1024]{1,0:T(8,128)(2,1)} fusion(f32[3072,1024]{1,0:T(8,128)} %fusion.3, f32[3072]{0:T(1024)S(1)} %bitcast.29, bf16[512,1024]{1,0:T(8,128)(2,1)S(1)} %bitcast.26, bf16[6144,512]{1,0:T(8,128)(2,1)} %all-gather.2.cloned.1.call-done), kind=kOutput, calls=%fused_computation | convolution fusion | flops 3230662656 | bytes 23080960 | tf_op jit(solution)/shard_map/dot_general | solution.py:50
  527.9 4.8 all-to-all-start.3
  532.7 25.0 %all-to-all-done.3 = bf16[2,512,1024]{2,1,0:T(8,128)(2,1)} async-done(((bf16[2,512,1024]{2,1,0:T(8,128)(2,1)}), bf16[2,512,1024]{2,1,0:T(8,128)(2,1)}, u32[]{:S(2)}, u32[]{:S(2)}) %all-to-all-start.3) | async-done | bytes 2097184 | tf_op jit(solution)/shard_map/all_to_all | solution.py:42
  557.7 4.0 copy.23
  561.7 3.9 copy.25
  565.7 32.1 %reduce-scatter.2.cloned.1.call-done = bf16[384,1024]{1,0:T(8,128)(2,1)} async-done(((bf16[3072,1024]{1,0:T(8,128)(2,1)}), bf16[384,1024]{1,0:T(8,128)(2,1)}) %reduce-scatter.2.cloned.1.call-update) | async-done | bytes 786448 | tf_op jit(solution)/shard_map/reduce_scatter | solution.py:56
  599.1 3.0 copy.29
  (14 shorter events, 4.1 us)
Async XLA Ops:
  14.0 55.4 %all-to-all-start = ((bf16[8,256,512]{2,1,0:T(8,128)(2,1)}), bf16[8,256,512]{2,1,0:T(8,128)(2,1)S(1)}, u32[]{:S(2)}, u32[]{:S(2)}) async-start(bf16[8,256,512]{2,1,0:T(8,128)(2,1)} %get-tuple-element.15), calls=%async_computation | async-start | bytes 4194304 | tf_op jit(solution)/shard_map/all_to_all | solution.py:30
  357.5 53.4 %all-to-all-start.1 = ((bf16[8,256,512]{2,1,0:T(8,128)(2,1)}), bf16[8,256,512]{2,1,0:T(8,128)(2,1)}, u32[]{:S(2)}, u32[]{:S(2)}) async-start(bf16[8,256,512]{2,1,0:T(8,128)(2,1)} %get-tuple-element.14), calls=%async_computation.1 | async-start | bytes 4194304 | tf_op jit(solution)/shard_map/all_to_all | solution.py:33
  361.9 144.2 %all-gather.2.cloned.1.call-start = ((), (), s32[]{:S(2)}) async-start(), calls=%async_computation.7 | async-start | bytes 9437184 | tf_op jit(solution)/shard_map/all_gather | solution.py:47
  426.6 8.3 %copy-start = (f32[384,4]{0,1:T(4,128)S(1)}, f32[384,4]{0,1:T(4,128)}, u32[]{:S(2)}) copy-start(f32[384,4]{0,1:T(4,128)} %param.9) | copy-start | bytes 18436
  426.7 8.3 %copy-start.1 = (s32[384,4]{0,1:T(4,128)S(1)}, s32[384,4]{0,1:T(4,128)}, u32[]{:S(2)}) copy-start(s32[384,4]{0,1:T(4,128)} %param.8) | copy-start | bytes 18436
  430.5 53.4 %all-to-all-start.2 = ((bf16[8,128,1024]{2,1,0:T(8,128)(2,1)}), bf16[8,128,1024]{2,1,0:T(8,128)(2,1)}, u32[]{:S(2)}, u32[]{:S(2)}) async-start(bf16[8,128,1024]{2,1,0:T(8,128)(2,1)} %convert_element_type.23), calls=%async_computation.2 | async-start | bytes 4194304 | tf_op jit(solution)/shard_map/all_to_all | solution.py:36
  483.9 32.3 %all-to-all-start.5 = ((f32[8,1,384]{2,1,0:T(1,128)}), f32[8,1,384]{2,1,0:T(1,128)S(1)}, u32[]{:S(2)}, u32[]{:S(2)}) async-start(f32[8,1,384]{2,1,0:T(1,128)} %copy.24), calls=%async_computation.5 | async-start | bytes 24576 | tf_op jit(solution)/shard_map/all_to_all | solution.py:23
  487.3 110.5 %reduce-scatter.2.cloned.1.call-start = ((), (), s32[]{:S(2)}) async-start(), calls=%async_computation.8 | async-start | bytes 7077888 | tf_op jit(solution)/shard_map/reduce_scatter | solution.py:56
  527.9 29.9 %all-to-all-start.3 = ((bf16[2,512,1024]{2,1,0:T(8,128)(2,1)}), bf16[2,512,1024]{2,1,0:T(8,128)(2,1)}, u32[]{:S(2)}, u32[]{:S(2)}) async-start(bf16[2,512,1024]{2,1,0:T(8,128)(2,1)} %bitcast.2), calls=%async_computation.3 | async-start | bytes 4194304 | tf_op jit(solution)/shard_map/all_to_all | solution.py:42
Sparse Core Ops, SparseCore 0:
  426.8 79.2 all-gather.1
  528.0 69.7 reduce-scatter.1
